TPU v7x, 32 devices: a whole 2x2x4 slice. The times are simulated.
32 devices in a mesh: ep: 8 (over z, y), tp: 4 (over x, core).
Axes of the slice: x: 2, y: 2, z: 4, core: 2. Of those that a mesh axis runs over, the one named last changes fastest.
Arguments:
- tokens: bfloat16 [24, 2048], P('ep'), may hold values from -6 to 6
- mixer_gain: float32 [2048], replicated, may hold values from 0.1 to 1.9
- query_weight: bfloat16 [2048, 2048], P('ep', 'tp'), may hold values from -0.125 to 0.125
- key_cache: bfloat16 [24, 1024, 4, 128], P('ep', None, 'tp'), may hold values from -6 to 6
- value_cache: bfloat16 [24, 1024, 4, 128], P('ep', None, 'tp'), may hold values from -6 to 6
- seq_lengths: int32 [24], P('ep'), may hold values from 1 to 1024, as said below
- head_offset: float32 [16], P('tp'), may hold values from -8.5 to -3.5
- output_weight: bfloat16 [2048, 2048], P('tp', 'ep'), may hold values from -0.5 to 0.5
- expert_gain: float32 [2048], replicated, may hold values from 0.1 to 1.9
- expert_ids: int32 [24, 2], P('ep'), may hold values from 0 to 7, as said below
- route_weight: float32 [24, 2], P('ep'), may hold values from 0.2 to 1
- gate_weight: bfloat16 [8, 2048, 1024], P('ep', None, 'tp'), may hold values from -0.125 to 0.125
- up_weight: bfloat16 [8, 2048, 1024], P('ep', None, 'tp'), may hold values from -0.125 to 0.125
- down_weight: bfloat16 [8, 1024, 2048], P('ep', 'tp'), may hold values from -0.1875 to 0.1875
Outputs:
- layer_out: bfloat16 [24, 2048], P('ep', 'tp')
Inputs may be any that keep to these rules, and one draw needn't show every extreme that they name: `seq_lengths`: some sequence holds all 1024 positions. `expert_ids`: the 2 experts of a row are different and lie in one group of 4 consecutive expert numbers. Among the 3 rows of one index of ep no expert is named by more than 2 rows, and some expert by exactly 2.
All inputs are finite; a program needn't handle non-finite values.
Results may differ from a plain program's by a relative error of at most 0.012.
Values may be sent and summed in bfloat16 or wider, within the bound.
A program may use at most 64 MiB of HBM per device.

v0:
```python
import jax
import jax.numpy as jnp
from jax import lax
from jax.sharding import PartitionSpec as P

EPG = 4
TOP = 2
BLK = 256


def rms_norm(values, gain):
    wide = values.astype(jnp.float32)
    scale = lax.rsqrt(jnp.mean(wide * wide, axis=-1, keepdims=True) + 1e-06)
    return (wide * scale * gain).astype(jnp.bfloat16)


def attend_cache(query, key_cache, value_cache, seq_lengths, head_offset):
    batch = query.shape[0]
    local_heads = head_offset.shape[0]
    kv_local = key_cache.shape[2]
    head_size = key_cache.shape[3]
    per_group = local_heads // kv_local
    grouped = query.reshape(batch, kv_local, per_group, head_size)
    offset = head_offset.reshape(1, kv_local, per_group, 1)
    scale = head_size ** (-0.5)
    longest = jnp.max(seq_lengths)
    block_count = (longest + BLK - 1) // BLK

    def step(turn, carry):
        total, later = carry
        start = (block_count - 1 - turn) * BLK
        keys = lax.dynamic_slice_in_dim(key_cache, start, BLK, 1)
        values = lax.dynamic_slice_in_dim(value_cache, start, BLK, 1)
        score = (
            jnp.einsum("bkgd,bskd->bkgs", grouped, keys, preferred_element_type=jnp.float32) * scale
            + offset
        )
        places = start + jnp.arange(BLK, dtype=jnp.int32)
        valid = (places[None, :] < seq_lengths[:, None])[:, None, None, :]
        log_take = jax.nn.log_sigmoid(score)
        log_pass = jnp.where(valid, jax.nn.log_sigmoid(-score), 0.0)
        inside = lax.cumsum(log_pass, axis=3, reverse=True) - log_pass + later[..., None]
        weight = jnp.where(valid, jnp.exp(log_take + inside), 0.0).astype(jnp.bfloat16)
        total = total + jnp.einsum(
            "bkgs,bskd->bkgd", weight, values, preferred_element_type=jnp.float32
        )
        return (total, later + jnp.sum(log_pass, axis=3))

    start_total = jnp.zeros((batch, kv_local, per_group, head_size), jnp.float32)
    start_later = jnp.zeros((batch, kv_local, per_group), jnp.float32)
    total, later = lax.fori_loop(0, block_count, step, (start_total, start_later))
    return total.reshape(batch, local_heads * head_size).astype(jnp.bfloat16)


def expert_hidden(rows, gate_weight, up_weight):
    gate = jnp.dot(rows, gate_weight[0], preferred_element_type=jnp.float32)
    upward = jnp.dot(rows, up_weight[0], preferred_element_type=jnp.float32)
    return (jax.nn.silu(gate) * upward).astype(jnp.bfloat16)


def local(
    tokens,
    mixer_gain,
    query_weight,
    key_cache,
    value_cache,
    seq_lengths,
    head_offset,
    output_weight,
    expert_gain,
    expert_ids,
    route_weight,
    gate_weight,
    up_weight,
    down_weight,
):
    ep_count = lax.axis_size("ep")
    batch = tokens.shape[0]
    normed = rms_norm(tokens, mixer_gain)
    feature_rows = lax.all_to_all(normed, "ep", split_axis=1, concat_axis=0, tiled=True)
    query = lax.psum_scatter(
        jnp.dot(feature_rows, query_weight, preferred_element_type=jnp.float32),
        "ep",
        scatter_dimension=0,
        tiled=True,
    )
    query = query.astype(jnp.bfloat16)
    mixed = attend_cache(query, key_cache, value_cache, seq_lengths, head_offset)
    partial_value = jnp.dot(
        lax.all_gather(mixed, "ep", axis=0, tiled=True),
        output_weight,
        preferred_element_type=jnp.float32,
    ).astype(jnp.bfloat16)
    summed = lax.psum(partial_value, "tp").astype(jnp.float32)
    attention = lax.all_to_all(summed, "ep", split_axis=0, concat_axis=1, tiled=True)
    resid = (tokens.astype(jnp.float32) + attention).astype(jnp.bfloat16)
    normed2 = rms_norm(resid, expert_gain)
    group_total = ep_count // EPG
    slot_count = max(2, (batch + group_total - 1) // group_total)
    pair_count = batch * TOP
    pair_ids = expert_ids.reshape(pair_count)
    order = jnp.arange(pair_count, dtype=jnp.int32)
    earlier = (order[None, :] < order[:, None]) & (pair_ids[:, None] == pair_ids[None, :])
    slot_index = jnp.sum(earlier.astype(jnp.int32), axis=1)
    dest_slot = pair_ids * slot_count + slot_index
    places = jnp.arange(ep_count * slot_count, dtype=jnp.int32)
    dispatch = (places[:, None] == dest_slot[None, :]).astype(jnp.bfloat16)
    pair_rows = jnp.repeat(normed2, TOP, axis=0)
    outgoing = jnp.dot(dispatch, pair_rows, preferred_element_type=jnp.float32).astype(jnp.bfloat16)
    outgoing = outgoing.reshape(ep_count, slot_count, normed2.shape[1])
    received = lax.all_to_all(outgoing, "ep", split_axis=0, concat_axis=0, tiled=True)
    count = received.shape[1]
    flat_rows = received.reshape(ep_count * count, received.shape[2])
    hidden = expert_hidden(flat_rows, gate_weight, up_weight)
    term = jnp.dot(hidden, down_weight[0], preferred_element_type=jnp.float32)
    reduced = lax.psum_scatter(term.astype(jnp.bfloat16), "tp", scatter_dimension=1, tiled=True)
    results = reduced.reshape(ep_count, count, reduced.shape[1])
    returned = lax.all_to_all(results, "ep", split_axis=0, concat_axis=0, tiled=True)
    columns = returned.shape[2]
    picked = jnp.dot(
        dispatch.T,
        returned.reshape(ep_count * slot_count, columns),
        preferred_element_type=jnp.float32,
    )
    weighted = picked.reshape(batch, TOP, columns) * route_weight[:, :, None]
    mixture = jnp.sum(weighted, axis=1)
    slice_width = mixture.shape[1]
    column_start = lax.axis_index("tp") * slice_width
    resid_slice = lax.dynamic_slice_in_dim(resid, column_start, slice_width, 1)
    return (resid_slice.astype(jnp.float32) + mixture).astype(jnp.bfloat16)


def solution(mesh):
    in_specs = (
        P("ep", None),
        P(),
        P("ep", "tp"),
        P("ep", None, "tp", None),
        P("ep", None, "tp", None),
        P("ep"),
        P("tp"),
        P("tp", "ep"),
        P(),
        P("ep", None),
        P("ep", None),
        P("ep", None, "tp"),
        P("ep", None, "tp"),
        P("ep", "tp", None),
    )
    out_specs = P("ep", "tp")
    return jax.shard_map(local, mesh=mesh, in_specs=in_specs, out_specs=out_specs, check_vma=False)
```

profile of v0, /device:TPU:0, one launch (start us, length us, event | category | flops | bytes accessed | tf_op | source)
XLA Modules:
  0.0 234.0 jit_solution(9833385639679030872)
XLA Ops:
  6.5 0.9 fusion.32
  7.5 1.4 fusion.34
  8.9 7.4 %all-to-all-start = ((bf16[3,8,256]{2,0,1:T(4,128)(2,1)}), bf16[3,8,256]{2,0,1:T(4,128)(2,1)S(1)}, u32[]{:S(2)}, u32[]{:S(2)}) async-start(bf16[3,8,256]{2,0,1:T(4,128)(2,1)} %bitcast.12), calls=%async_computation | async-start | bytes 32768 | tf_op jit(solution)/shard_map/all_to_all | solution.py:80
  16.5 0.2 convert_reduce_fusion
  16.7 0.5 copy-done.5
  17.2 0.6 reduce_max.9
  18.5 0.6 copy-done.10
  19.1 0.6 dynamic-slice
  20.4 2.5 %all-to-all-done = bf16[3,8,256]{2,0,1:T(4,128)(2,1)S(1)} async-done(((bf16[3,8,256]{2,0,1:T(4,128)(2,1)}), bf16[3,8,256]{2,0,1:T(4,128)(2,1)S(1)}, u32[]{:S(2)}, u32[]{:S(2)}) %all-to-all-start) | async-done | bytes 12320 | tf_op jit(solution)/shard_map/all_to_all | solution.py:80
  22.9 1.1 fusion.49
  24.0 35.5 %all-reduce = bf16[24,512]{1,0:T(8,128)(2,1)S(1)} all-reduce(f32[24,512]{1,0:T(8,128)S(1)} %fusion.49), channel_id=2, replica_groups=mesh['ep'=8,'tp'=4] {'ep'}, use_global_device_ids=true, to_apply=%region_2.0.clone | all-reduce | flops 12288 | bytes 73728
  59.6 0.6 copy-done.9
  60.3 72.1 %while.14 = (s32[]{:T(128)}, f32[3,1,4,128]{3,2,0,1:T(4,128)S(1)}, f32[3,1,4]{2,0,1:T(4,128)S(1)}, s32[]{:T(128)}, s32[]{:T(128)}, /*index=5*/s32[3]{0:T(128)S(1...) while((s32[]{:T(128)}, f32[3,1,4,128]{3,2,0,1:T(4,128)S(1)}, ...), condition=%wide.region_7.8_spmd, body=%wide.region_3.7_spmd.sunk | while | flops 2042411 | bytes 598647 | solution.py:51
  60.3 1.2 fusion.64
  61.6 15.1 %reduce-window.16 = f32[3,1,4,2,128]{4,3,2,1,0:T(2,128)S(1)} reduce-window(f32[3,1,4,2,128]{4,3,2,1,0:T(2,128)S(1)} %bitcast.80, f32[]{:T(128)} %constant.65.clone.1..sunk), window={size=1x1x1x1x128 pad=0_0x0_0x0_0x0_0x0_127}, to_apply=%region_4.4 | reduce-window | flops 390144 | bytes 24580 | tf_op jit(solution)/shard_map/reduce-window.4
  76.7 0.1 copy.51
  76.9 0.1 copy.52
  77.1 1.1 fusion.65
  78.4 1.2 fusion.64
  79.6 15.1 %reduce-window.16 = f32[3,1,4,2,128]{4,3,2,1,0:T(2,128)S(1)} reduce-window(f32[3,1,4,2,128]{4,3,2,1,0:T(2,128)S(1)} %bitcast.80, f32[]{:T(128)} %constant.65.clone.1..sunk), window={size=1x1x1x1x128 pad=0_0x0_0x0_0x0_0x0_127}, to_apply=%region_4.4 | reduce-window | flops 390144 | bytes 24580 | tf_op jit(solution)/shard_map/reduce-window.4
  94.7 0.1 copy.51
  95.1 1.1 fusion.65
  96.4 1.2 fusion.64
  97.6 15.1 %reduce-window.16 = f32[3,1,4,2,128]{4,3,2,1,0:T(2,128)S(1)} reduce-window(f32[3,1,4,2,128]{4,3,2,1,0:T(2,128)S(1)} %bitcast.80, f32[]{:T(128)} %constant.65.clone.1..sunk), window={size=1x1x1x1x128 pad=0_0x0_0x0_0x0_0x0_127}, to_apply=%region_4.4 | reduce-window | flops 390144 | bytes 24580 | tf_op jit(solution)/shard_map/reduce-window.4
  112.7 0.1 copy.51
  112.9 0.1 copy.52
  113.1 1.1 fusion.65
  114.4 1.2 fusion.64
  115.6 15.1 %reduce-window.16 = f32[3,1,4,2,128]{4,3,2,1,0:T(2,128)S(1)} reduce-window(f32[3,1,4,2,128]{4,3,2,1,0:T(2,128)S(1)} %bitcast.80, f32[]{:T(128)} %constant.65.clone.1..sunk), window={size=1x1x1x1x128 pad=0_0x0_0x0_0x0_0x0_127}, to_apply=%region_4.4 | reduce-window | flops 390144 | bytes 24580 | tf_op jit(solution)/shard_map/reduce-window.4
  130.8 0.1 copy.51
  130.9 0.1 copy.52
  131.2 1.1 fusion.65
  132.4 30.7 %all-gather = bf16[8,3,512]{2,1,0:T(4,128)(2,1)S(1)} all-gather(bf16[1,3,512]{2,1,0:T(4,128)(2,1)S(1)} %reshape.218), channel_id=1, replica_groups=mesh['ep'=8,'tp'=4] {'ep'}, dimensions={0}, use_global_device_ids=true | all-gather | bytes 27648 | tf_op jit(solution)/shard_map/all_gather | solution.py:90
  163.2 0.2 convolution_convert_fusion.2
  163.3 10.3 %psum.7 = bf16[8,3,256]{2,1,0:T(4,128)(2,1)S(1)} all-reduce(bf16[8,3,256]{2,1,0:T(4,128)(2,1)S(1)} %all_to_all.40), channel_id=1, replica_groups=mesh['ep'=8,'tp'=4] {'tp'}, use_global_device_ids=true, to_apply=%region_8.9 | all-reduce | flops 6144 | bytes 24576 | tf_op jit(solution)/shard_map/psum | solution.py:94
  173.6 0.6 all_to_all.41
  174.2 3.3 %all-to-all-start.1 = ((f32[8,3,256]{2,1,0:T(4,128)}), f32[8,3,256]{2,1,0:T(4,128)S(1)}, u32[]{:S(2)}, u32[]{:S(2)}) async-start(f32[8,3,256]{2,1,0:T(4,128)} %all_to_all.41), calls=%async_computation.1 | async-start | bytes 65536 | tf_op jit(solution)/shard_map/all_to_all | solution.py:95
  177.6 6.6 %all-to-all-done.1 = f32[8,3,256]{2,1,0:T(4,128)S(1)} async-done(((f32[8,3,256]{2,1,0:T(4,128)}), f32[8,3,256]{2,1,0:T(4,128)S(1)}, u32[]{:S(2)}, u32[]{:S(2)}) %all-to-all-start.1) | async-done | bytes 24608 | tf_op jit(solution)/shard_map/all_to_all | solution.py:95
  184.2 0.1 fusion.29
  184.4 0.1 convolution_convert_fusion.1
  184.6 9.3 %all_to_all.51 = bf16[8,2,2048]{2,1,0:T(2,128)(2,1)S(1)} all-to-all(bf16[8,2,2048]{2,1,0:T(2,128)(2,1)S(1)} %reshape.214), channel_id=1, replica_groups=mesh['ep'=8,'tp'=4] {'ep'}, dimensions={0} | all-to-all | bytes 131072 | tf_op jit(solution)/shard_map/all_to_all | solution.py:111
  194.0 0.2 fusion.27
  194.2 1.4 convolution_convert_fusion
  195.6 17.3 %reduce-scatter.2.cloned.1.call-done = bf16[16,512]{1,0:T(8,128)(2,1)} async-done(((bf16[16,2048]{1,0:T(8,128)(2,1)}), bf16[16,512]{1,0:T(8,128)(2,1)}) %reduce-scatter.2.cloned.1.call-update) | async-done | bytes 16400 | tf_op jit(solution)/shard_map/reduce_scatter | solution.py:116
  212.9 1.3 reshape.216
  214.3 5.5 %all-to-all-start.3 = ((bf16[8,2,512]{2,1,0:T(2,128)(2,1)}), bf16[8,2,512]{2,1,0:T(2,128)(2,1)S(1)}, u32[]{:S(2)}, u32[]{:S(2)}) async-start(bf16[8,2,512]{2,1,0:T(2,128)(2,1)} %reshape.216), calls=%async_computation.4 | async-start | bytes 32768 | tf_op jit(solution)/shard_map/all_to_all | solution.py:118
  219.9 6.5 %all-to-all-done.3 = bf16[8,2,512]{2,1,0:T(2,128)(2,1)S(1)} async-done(((bf16[8,2,512]{2,1,0:T(2,128)(2,1)}), bf16[8,2,512]{2,1,0:T(2,128)(2,1)S(1)}, u32[]{:S(2)}, u32[]{:S(2)}) %all-to-all-start.3) | async-done | bytes 16416 | tf_op jit(solution)/shard_map/all_to_all | solution.py:118
  226.5 0.7 add_convert_fusion
  (81 shorter events, 2.0 us)
Async XLA Ops:
  6.5 187.7 %copy-start = (bf16[1,256,2048]{2,1,0:T(8,128)(2,1)S(1)}, bf16[1,256,2048]{2,1,0:T(8,128)(2,1)}, u32[]{:S(2)}) copy-start(bf16[1,256,2048]{2,1,0:T(8,128)(2,1)} %param.29) | copy-start | bytes 3145732
  6.5 1.0 copy-start.4
  8.9 7.4 %copy-start.7 = (s32[3,2]{0,1:T(2,128)S(1)}, s32[3,2]{0,1:T(2,128)}, u32[]{:S(2)}) copy-start(s32[3,2]{0,1:T(2,128)} %param.25) | copy-start | bytes 76
  8.9 14.0 %all-to-all-start = ((bf16[3,8,256]{2,0,1:T(4,128)(2,1)}), bf16[3,8,256]{2,0,1:T(4,128)(2,1)S(1)}, u32[]{:S(2)}, u32[]{:S(2)}) async-start(bf16[3,8,256]{2,0,1:T(4,128)(2,1)} %bitcast.12), calls=%async_computation | async-start | bytes 32768 | tf_op jit(solution)/shard_map/all_to_all | solution.py:80
  16.5 0.7 copy-start.5
  18.5 0.7 copy-start.10
  59.6 0.7 copy-start.9
  60.3 102.9 %copy-start.3 = (bf16[512,256]{1,0:T(8,128)(2,1)S(1)}, bf16[512,256]{1,0:T(8,128)(2,1)}, u32[]{:S(2)}) copy-start(bf16[512,256]{1,0:T(8,128)(2,1)} %param.23) | copy-start | bytes 786436
  60.3 124.0 %copy-start.6 = (f32[2048]{0:T(1024)S(1)}, f32[2048]{0:T(1024)}, u32[]{:S(2)}) copy-start(f32[2048]{0:T(1024)} %param.24) | copy-start | bytes 24580
  132.3 61.6 %copy-start.1 = (bf16[1,2048,256]{2,1,0:T(8,128)(2,1)S(1)}, bf16[1,2048,256]{2,1,0:T(8,128)(2,1)}, u32[]{:S(2)}) copy-start(bf16[1,2048,256]{2,1,0:T(8,128)(2,1)} %param.27) | copy-start | bytes 3145732
  163.3 30.9 %copy-start.2 = (bf16[1,2048,256]{2,1,0:T(8,128)(2,1)S(1)}, bf16[1,2048,256]{2,1,0:T(8,128)(2,1)}, u32[]{:S(2)}) copy-start(bf16[1,2048,256]{2,1,0:T(8,128)(2,1)} %param.28) | copy-start | bytes 3145732
  174.2 10.0 %all-to-all-start.1 = ((f32[8,3,256]{2,1,0:T(4,128)}), f32[8,3,256]{2,1,0:T(4,128)S(1)}, u32[]{:S(2)}, u32[]{:S(2)}) async-start(f32[8,3,256]{2,1,0:T(4,128)} %all_to_all.41), calls=%async_computation.1 | async-start | bytes 65536 | tf_op jit(solution)/shard_map/all_to_all | solution.py:95
  177.5 35.4 %reduce-scatter.2.cloned.1.call-start = ((), (), s32[]{:S(2)}) async-start(), calls=%async_computation.5 | async-start | bytes 81920 | tf_op jit(solution)/shard_map/reduce_scatter | solution.py:116
  214.3 12.1 %all-to-all-start.3 = ((bf16[8,2,512]{2,1,0:T(2,128)(2,1)}), bf16[8,2,512]{2,1,0:T(2,128)(2,1)S(1)}, u32[]{:S(2)}, u32[]{:S(2)}) async-start(bf16[8,2,512]{2,1,0:T(2,128)(2,1)} %reshape.216), calls=%async_computation.4 | async-start | bytes 32768 | tf_op jit(solution)/shard_map/all_to_all | solution.py:118
  219.9 6.5 %copy-start.8 = (f32[3,2]{0,1:T(2,128)S(1)}, f32[3,2]{0,1:T(2,128)}, u32[]{:S(2)}) copy-start(f32[3,2]{0,1:T(2,128)} %param.26) | copy-start | bytes 76
Sparse Core Ops, SparseCore 0:
  195.7 17.1 reduce-scatter.1
where the time goes:
time: 235 us; the launch traced here: 234 us
  blocking collectives  85.8 us (37%)
  other arithmetic  65.7 us (28%)
  waiting for transfers between devices  32.9 us (14%)
  starting transfers between devices  16.3 us (7%)
  between operations  14.9 us (6%)
  matrix products  12.5 us (5%)
  local copies, waits for them, and re-layouts  5.75 us (2%)
    another operation x8, other arithmetic  60.6 us
    unnamed x1, blocking collectives  35.5 us
    all_gather x1, blocking collectives, local(): lax.all_gather(mixed, 'ep', axis=0, tiled=True)  30.7 us
    reduce_scatter x1, waiting for transfers between devices, local(): lax.psum_scatter(term.astype(jnp.bfloat16), 'tp', scatter_dimension=1, ti...  17.3 us
    psum x1, blocking collectives, local(): summed = lax.psum(partial_value, 'tp').astype(jnp.float32)  10.3 us
    all_to_all x1, blocking collectives, local(): lax.all_to_all(outgoing, 'ep', split_axis=0, concat_axis=0, tiled=True)  9.29 us
    all_to_all x1, starting transfers between devices, local(): lax.all_to_all(normed, 'ep', split_axis=1, concat_axis=0, tiled=True)  7.44 us
    all_to_all x1, waiting for transfers between devices, local(): lax.all_to_all(summed, 'ep', split_axis=0, concat_axis=1, tiled=True)  6.56 us
  transfers between devices with their start and end apart: 4, of which 4 were waited for; matrix products, arithmetic and copies ran while one was open for 1% of the time, Pallas kernels for 0%

commit v1 on v0

--- a/solution.py
+++ b/solution.py
@@ -1,6 +1,8 @@
 import jax
 import jax.numpy as jnp
 from jax import lax
+from jax.experimental import pallas as pl
+from jax.experimental.pallas import tpu as pltpu
 from jax.sharding import PartitionSpec as P
 
 EPG = 4
@@ -58,7 +60,7 @@
     return (jax.nn.silu(gate) * upward).astype(jnp.bfloat16)
 
 
-def local(
+def local_collectives(
     tokens,
     mixer_gain,
     query_weight,
@@ -130,6 +132,376 @@
     return (resid_slice.astype(jnp.float32) + mixture).astype(jnp.bfloat16)
 
 
+MESH = pl.DeviceIdType.MESH
+LANES = 128
+SUBLANES = 8
+
+
+def wait_bytes(ref, count, sem):
+    view = ref.at[pl.ds(0, count)]
+    pltpu.make_async_copy(view, view, sem).wait()
+
+
+def layer_kernel(
+    ep,
+    tp,
+    tokens_ref,
+    mixer_gain_ref,
+    expert_gain_ref,
+    lengths_ref,
+    offset_ref,
+    ids_ref,
+    route_ref,
+    query_hbm,
+    key_hbm,
+    value_hbm,
+    output_hbm,
+    gate_hbm,
+    up_hbm,
+    down_hbm,
+    out_ref,
+    query_w,
+    key_w,
+    value_w,
+    output_w,
+    gate_w,
+    up_w,
+    down_w,
+    load_sem,
+    send_sem,
+    recv_sem,
+    a_send,
+    a_recv,
+    b_send,
+    b_recv,
+    c_send,
+    c_recv,
+    d_send,
+    d_recv,
+    e_send,
+    e_recv,
+    f_send,
+    f_recv,
+    rows_s,
+    token_s,
+    part_s,
+    query_s,
+    mixed_s,
+    mixed_rows_s,
+    resid_s,
+    term_s,
+):
+    me, mt = lax.axis_index("ep"), lax.axis_index("tp")
+    total = ep * tp
+    flat = me * tp + mt
+    batch, width = tokens_ref.shape
+    cols = query_w.shape[0]
+    heads = offset_ref.shape[0]
+    head_size = mixed_s.shape[1] // heads
+    cache = key_w.shape[1]
+    kv_local = key_w.shape[2] // head_size
+    per_group = heads // kv_local
+    out_cols = out_ref.shape[1]
+    f32, bf16 = jnp.float32, jnp.bfloat16
+
+    loads = []
+    for place, (source, target) in enumerate(
+        (
+            (query_hbm, query_w),
+            (key_hbm, key_w),
+            (value_hbm, value_w),
+            (output_hbm, output_w),
+            (gate_hbm, gate_w),
+            (up_hbm, up_w),
+            (down_hbm, down_w),
+        )
+    ):
+        loads.append(pltpu.make_async_copy(source, target, load_sem.at[place]))
+        loads[-1].start()
+
+    barrier = pltpu.get_barrier_semaphore()
+    for step in range(1, total):
+        other = lax.rem(flat + step, total)
+        pl.semaphore_signal(
+            barrier, inc=1, device_id=(other // tp, lax.rem(other, tp)), device_id_type=MESH
+        )
+
+    def send(phase, source, target, device):
+        pltpu.make_async_remote_copy(
+            src_ref=source,
+            dst_ref=target,
+            send_sem=send_sem.at[phase],
+            recv_sem=recv_sem.at[phase],
+            device_id=device,
+            device_id_type=MESH,
+        ).start()
+
+    def ep_peers():
+        return [lax.rem(me + step, ep) for step in range(1, ep)]
+
+    wide = tokens_ref[...].astype(f32)
+    scale = lax.rsqrt(jnp.mean(wide * wide, axis=-1, keepdims=True) + 1e-06)
+    normed = wide * scale * mixer_gain_ref[...]
+    for e in range(ep):
+        a_send[e, 0] = normed[:, e * cols : (e + 1) * cols].astype(bf16)
+        a_send[e, 1] = tokens_ref[:, e * cols : (e + 1) * cols]
+    query_s[...] = jnp.zeros_like(query_s)
+    pl.semaphore_wait(barrier, total - 1)
+    for peer in ep_peers():
+        send(0, a_send.at[peer], a_recv.at[me], (peer, mt))
+    a_recv[me] = a_send[me]
+
+    earlier = lax.broadcasted_iota(jnp.int32, (LANES, 2 * LANES), 0)
+    later = lax.broadcasted_iota(jnp.int32, (LANES, 2 * LANES), 1)
+    suffix = ((earlier > later) | (later >= LANES)).astype(f32).astype(bf16)
+    suffix = jnp.concatenate([suffix] * 3, axis=0)
+
+    loads[0].wait()
+    wait_bytes(a_recv, ep - 1, recv_sem.at[0])
+    for e in range(ep):
+        rows_s[batch * e : batch * (e + 1), :] = a_recv[e, 0].astype(f32)
+        token_s[batch * e : batch * (e + 1), :] = a_recv[e, 1].astype(f32)
+    part_s[...] = jnp.dot(rows_s[...].astype(bf16), query_w[...], preferred_element_type=f32)
+    for e in range(ep):
+        b_send[e] = part_s[batch * e : batch * (e + 1), :]
+    for peer in ep_peers():
+        send(1, b_send.at[peer], b_recv.at[me], (peer, mt))
+    b_recv[me] = b_send[me]
+    loads[1].wait()
+    loads[2].wait()
+    wait_bytes(b_recv, ep - 1, recv_sem.at[1])
+    query = b_recv[0]
+    for e in range(1, ep):
+        query = query + b_recv[e]
+    query = query.astype(bf16).astype(f32)
+
+    groups = [(row, kv) for row in range(batch) for kv in range(kv_local)]
+    places = lax.broadcasted_iota(jnp.int32, (SUBLANES, cache), 1)
+    line = lax.broadcasted_iota(jnp.int32, (SUBLANES, 1), 0)
+    blocks = cache // LANES
+    takes, passes, valids = [], [], []
+    for row, kv in groups:
+        offset = jnp.zeros((SUBLANES, 1), f32)
+        for h in range(per_group):
+            head = kv * per_group + h
+            query_s[row, kv, h : h + 1, :] = query[
+                row : row + 1, head * head_size : (head + 1) * head_size
+            ]
+            offset = jnp.where(line == h, offset_ref[head], offset)
+        keys = key_w[row, :, kv * head_size : (kv + 1) * head_size]
+        score = lax.dot_general(
+            query_s[row, kv].astype(bf16),
+            keys,
+            (((1,), (1,)), ((), ())),
+            preferred_element_type=f32,
+        )
+        score = score * (head_size ** (-0.5)) + offset
+        valid = places < lengths_ref[row]
+        soft = jnp.log1p(jnp.exp(-jnp.abs(score)))
+        takes.append(jnp.minimum(score, 0.0) - soft)
+        passes.append(jnp.where(valid, jnp.minimum(-score, 0.0) - soft, 0.0))
+        valids.append(valid)
+    tall = jnp.concatenate(
+        [p[:, j * LANES : (j + 1) * LANES] for p in passes for j in range(blocks)], axis=0
+    )
+    high = tall.astype(bf16)
+    rest = tall - high.astype(f32)
+    middle = rest.astype(bf16)
+    low = (rest - middle.astype(f32)).astype(bf16)
+    sums = jnp.dot(
+        jnp.concatenate([high, middle, low], axis=1), suffix, preferred_element_type=f32
+    )
+    for at, (row, kv) in enumerate(groups):
+        carry = jnp.zeros((SUBLANES, LANES), f32)
+        inside = [None] * blocks
+        for j in reversed(range(blocks)):
+            top = (at * blocks + j) * SUBLANES
+            inside[j] = sums[top : top + SUBLANES, :LANES] + carry
+            carry = carry + sums[top : top + SUBLANES, LANES:]
+        weight = jnp.where(
+            valids[at], jnp.exp(takes[at] + jnp.concatenate(inside, axis=1)), 0.0
+        ).astype(bf16)
+        values = value_w[row, :, kv * head_size : (kv + 1) * head_size]
+        mixed = jnp.dot(weight, values, preferred_element_type=f32)
+        for h in range(per_group):
+            head = kv * per_group + h
+            mixed_s[row : row + 1, head * head_size : (head + 1) * head_size] = mixed[h : h + 1, :]
+    c_send[...] = mixed_s[...].astype(bf16)
+    for peer in ep_peers():
+        send(2, c_send, c_recv.at[me], (peer, mt))
+    c_recv[me] = c_send[...]
+    loads[3].wait()
+    wait_bytes(c_recv, ep - 1, recv_sem.at[2])
+    for e in range(ep):
+        mixed_rows_s[batch * e : batch * (e + 1), :] = c_recv[e].astype(f32)
+
+    d_send[...] = jnp.dot(
+        mixed_rows_s[...].astype(bf16), output_w[...], preferred_element_type=f32
+    ).astype(bf16)
+    for step in range(1, tp):
+        send(3, d_send, d_recv.at[mt], (me, lax.rem(mt + step, tp)))
+    d_recv[mt] = d_send[...]
+    wait_bytes(d_recv, tp - 1, recv_sem.at[3])
+    resid = token_s[...]
+    for t in range(tp):
+        resid = resid + d_recv[t].astype(f32)
+    e_send[...] = resid.astype(bf16)
+
+    for peer in ep_peers():
+        send(4, e_send, e_recv.at[me], (peer, mt))
+    e_recv[me] = e_send[...]
+    numbers = ids_ref[...]
+    routes = route_ref[...]
+    shares = [
+        jnp.sum(jnp.where(numbers == e, routes, 0.0), axis=1, keepdims=True) for e in range(ep)
+    ]
+    loads[4].wait()
+    loads[5].wait()
+    loads[6].wait()
+    wait_bytes(e_recv, ep - 1, recv_sem.at[4])
+    square = None
+    for e in range(ep):
+        block = e_recv[e].astype(f32)
+        resid_s[e] = block
+        square = block * block if square is None else square + block * block
+    scale = lax.rsqrt(jnp.sum(square, axis=-1, keepdims=True) / width + 1e-06)
+    normed2 = jnp.concatenate(
+        [
+            (resid_s[e] * scale * expert_gain_ref[:, e * cols : (e + 1) * cols]).astype(bf16)
+            for e in range(ep)
+        ],
+        axis=1,
+    )
+    gate = jnp.dot(normed2, gate_w[0], preferred_element_type=f32)
+    upward = jnp.dot(normed2, up_w[0], preferred_element_type=f32)
+    hidden = (gate / (1.0 + jnp.exp(-gate)) * upward).astype(bf16)
+    term_s[...] = jnp.dot(hidden, down_w[0], preferred_element_type=f32)
+    for e in range(ep):
+        for t in range(tp):
+            f_send[e * tp + t] = term_s[
+                batch * e : batch * (e + 1), t * out_cols : (t + 1) * out_cols
+            ].astype(bf16)
+    for step in range(1, total):
+        other = lax.rem(flat + step, total)
+        send(5, f_send.at[other], f_recv.at[flat], (other // tp, lax.rem(other, tp)))
+    f_recv[flat] = f_send[flat]
+    own_blocks = out_cols // cols
+    row_at = lax.broadcasted_iota(jnp.int32, (batch, ep * batch), 0) + me * batch
+    column_at = lax.broadcasted_iota(jnp.int32, (batch, ep * batch), 1)
+    own_rows = (row_at == column_at).astype(f32).astype(bf16)
+    own_resid = jnp.concatenate(
+        [e_recv[mt * own_blocks + j] for j in range(own_blocks)], axis=1
+    )
+    result = jnp.dot(own_rows, own_resid, preferred_element_type=f32)
+    wait_bytes(f_recv, total - 1, recv_sem.at[5])
+    mixture = jnp.zeros_like(result)
+    for e in range(ep):
+        summed = f_recv[e * tp].astype(f32)
+        for t in range(1, tp):
+            summed = summed + f_recv[e * tp + t].astype(f32)
+        mixture = mixture + summed.astype(bf16).astype(f32) * shares[e]
+    out_ref[...] = (result + mixture).astype(bf16)
+
+    wait_bytes(a_recv, ep - 1, send_sem.at[0])
+    wait_bytes(b_recv, ep - 1, send_sem.at[1])
+    wait_bytes(c_recv, ep - 1, send_sem.at[2])
+    wait_bytes(d_recv, tp - 1, send_sem.at[3])
+    wait_bytes(e_recv, ep - 1, send_sem.at[4])
+    wait_bytes(f_recv, total - 1, send_sem.at[5])
+
+
+def local_kernel(
+    tokens,
+    mixer_gain,
+    query_weight,
+    key_cache,
+    value_cache,
+    seq_lengths,
+    head_offset,
+    output_weight,
+    expert_gain,
+    expert_ids,
+    route_weight,
+    gate_weight,
+    up_weight,
+    down_weight,
+):
+    ep, tp = lax.axis_size("ep"), lax.axis_size("tp")
+    batch, width = tokens.shape
+    cols, heads_width = query_weight.shape
+    out_cols = width // tp
+    rows = ep * batch
+    heads = head_offset.shape[0]
+    cache, kv_local, head_size = key_cache.shape[1:]
+    keys = key_cache.reshape(batch, cache, kv_local * head_size)
+    values = value_cache.reshape(batch, cache, kv_local * head_size)
+    big = (query_weight, keys, values, output_weight, gate_weight, up_weight, down_weight)
+    f32, bf16 = jnp.float32, jnp.bfloat16
+    vmem = pl.BlockSpec(memory_space=pltpu.VMEM)
+    smem = pl.BlockSpec(memory_space=pltpu.SMEM)
+    hbm = pl.BlockSpec(memory_space=pl.ANY)
+
+    def body(*refs):
+        layer_kernel(ep, tp, *refs)
+
+    return pl.pallas_call(
+        body,
+        out_shape=jax.ShapeDtypeStruct((batch, out_cols), bf16),
+        in_specs=[vmem, vmem, vmem, smem, smem, vmem, vmem] + [hbm] * len(big),
+        out_specs=vmem,
+        scratch_shapes=[pltpu.VMEM(array.shape, array.dtype) for array in big]
+        + [
+            pltpu.SemaphoreType.DMA((len(big),)),
+            pltpu.SemaphoreType.DMA((6,)),
+            pltpu.SemaphoreType.DMA((6,)),
+            pltpu.VMEM((ep, 2, batch, cols), bf16),
+            pltpu.VMEM((ep, 2, batch, cols), bf16),
+            pltpu.VMEM((ep, batch, heads_width), f32),
+            pltpu.VMEM((ep, batch, heads_width), f32),
+            pltpu.VMEM((batch, heads_width), bf16),
+            pltpu.VMEM((ep, batch, heads_width), bf16),
+            pltpu.VMEM((rows, cols), bf16),
+            pltpu.VMEM((tp, rows, cols), bf16),
+            pltpu.VMEM((rows, cols), bf16),
+            pltpu.VMEM((ep, rows, cols), bf16),
+            pltpu.VMEM((ep * tp, batch, out_cols), bf16),
+            pltpu.VMEM((ep * tp, batch, out_cols), bf16),
+            pltpu.VMEM((rows, cols), f32),
+            pltpu.VMEM((rows, cols), f32),
+            pltpu.VMEM((rows, heads_width), f32),
+            pltpu.VMEM((batch, kv_local, SUBLANES, head_size), f32),
+            pltpu.VMEM((batch, heads_width), f32),
+            pltpu.VMEM((rows, heads_width), f32),
+            pltpu.VMEM((ep, rows, cols), f32),
+            pltpu.VMEM((rows, width), f32),
+        ],
+        compiler_params=pltpu.CompilerParams(
+            collective_id=0, has_side_effects=True, vmem_limit_bytes=60 * 1024 * 1024
+        ),
+    )(
+        tokens,
+        mixer_gain.reshape(1, width),
+        expert_gain.reshape(1, width),
+        seq_lengths,
+        head_offset,
+        expert_ids,
+        route_weight,
+        *big,
+    )
+
+
+def local(*arrays):
+    tokens, query_weight = arrays[0], arrays[2]
+    key_cache, head_offset = arrays[3], arrays[6]
+    cols = query_weight.shape[0]
+    out_cols = tokens.shape[1] // lax.axis_size("tp")
+    cache, kv_local, head_size = key_cache.shape[1:]
+    whole_tiles = cols % LANES == 0 and head_size % LANES == 0 and cache % LANES == 0
+    if whole_tiles and out_cols % cols == 0 and head_offset.shape[0] // kv_local <= SUBLANES:
+        return local_kernel(*arrays)
+    return local_collectives(*arrays)
+
+
 def solution(mesh):
     in_specs = (
         P("ep", None),

time: 235 us -> 37.3 us (0.16)
  blocking collectives: 85.8 us -> 0 us
  other arithmetic: 65.7 us -> 0 us
  Pallas kernels: 0 us -> 33.7 us
  waiting for transfers between devices: 32.9 us -> 0 us
  starting transfers between devices: 16.3 us -> 0 us
  between operations: 14.9 us -> 0.01 us
  matrix products: 12.5 us -> 0 us
  local copies, waits for them, and re-layouts: 5.75 us -> 3.28 us
    another operation x8 -> x0, other arithmetic: 60.6 us -> none
    unnamed x1 -> x0, blocking collectives: 35.5 us -> none
    pallas_call x0 -> x1, Pallas kernels: none -> 33.7 us  [local_kernel(): pl.pallas_call(body, out_shape=jax.ShapeDtypeStruct((batch, out_cols), bf...]
    all_gather x1 -> x0, blocking collectives: 30.7 us -> none  [local(): lax.all_gather(mixed, 'ep', axis=0, tiled=True)]
    reduce_scatter x1 -> x0, waiting for transfers between devices: 17.3 us -> none  [local(): lax.psum_scatter(term.astype(jnp.bfloat16), 'tp', scatter_dimension=1, ti...]
    all_to_all x3 -> x0, starting transfers between devices: 16.3 us -> none  [the longest x1 7.44 us: local(): lax.all_to_all(normed, 'ep', split_axis=1, concat_axis=0, tiled=True)]
    all_to_all x3 -> x0, waiting for transfers between devices: 15.5 us -> none  [the longest x1 6.56 us: local(): lax.all_to_all(summed, 'ep', split_axis=0, concat_axis=1, tiled=True)]
    dot_general x14 -> x0, matrix products: 12.5 us -> none  [the longest x4 4.84 us: step(): jnp.einsum('bkgd,bskd->bkgs', grouped, keys, preferred_element_type=jnp.f...]
  transfers between devices with their start and end apart: 4 -> 0, of which waited for: 4 -> 0; matrix products, arithmetic and copies ran while one was open for 1% -> 0% of each run, Pallas kernels for 0% -> 0%
where the time goes in v1:
time: 37.3 us; the launch traced here: 37 us
  Pallas kernels  33.7 us (90%)
  local copies, waits for them, and re-layouts  3.28 us (9%)
    pallas_call x1, Pallas kernels, local_kernel(): pl.pallas_call(body, out_shape=jax.ShapeDtypeStruct((batch, out_cols), bf...  33.7 us
    unnamed x7, local copies, waits for them, and re-layouts  3.28 us

profile of v1, /device:TPU:0, one launch (start us, length us, event | category | flops | bytes accessed | tf_op | source)
XLA Modules:
  0.0 37.0 jit_solution(7480846973655481870)
XLA Ops:
  0.0 0.0 copy-start
  0.0 0.7 %copy-done = s32[3,2]{0,1:T(2,128)S(1)} copy-done((s32[3,2]{0,1:T(2,128)S(1)}, s32[3,2]{0,1:T(2,128)}, u32[]{:S(2)}) %copy-start) | copy-done | bytes 48
  0.7 0.0 copy-start.1
  0.7 0.7 %copy.15.refs_5_ = s32[3,2]{1,0:T(4,128)} copy(s32[3,2]{0,1:T(2,128)S(1)} %copy-done) | data formatting | bytes 48 | tf_op args[9]
  1.3 0.0 copy-done.1
  1.4 0.7 %copy.16.refs_6_ = f32[3,2]{1,0:T(4,128)} copy(f32[3,2]{0,1:T(2,128)S(1)} %copy-done.1) | data formatting | bytes 48 | tf_op args[10]
  2.0 33.7 %shard_map.136 = bf16[3,512]{1,0:T(4,128)(2,1)} custom-call(bf16[3,2048]{1,0:T(4,128)(2,1)} %refs_0_.1, f32[1,2048]{1,0:T(1,128)} %bitcast.6, f32[1,2048]{1,0:T(1,128)} %bitcast.7, s32[3]{0:T(128)} %refs_3_.1, f32[4]{0:T(128)} %refs_4_.1, s32[3,2]{1,0:T(4,128)} %copy.15.refs_5_, f32[3,2]{1,0:T(4,128)} %copy.16.refs_6_, bf16[256,512]{1,0:T(8,128)(2,1)} %refs_7_.1, ...), custom_call_target="tpu_custom_call" | custom-call | tf_op jit(solution)/shard_map/pallas_call | solution.py:447
  35.8 1.3 %copy.18 = bf16[3,512]{1,0:T(4,128)(2,1)} copy(bf16[3,512]{1,0:T(4,128)(2,1)} %shard_map.136) | data formatting | bytes 6144
Async XLA Ops:
  0.0 0.7 %copy-start = (s32[3,2]{0,1:T(2,128)S(1)}, s32[3,2]{0,1:T(2,128)}, u32[]{:S(2)}) copy-start(s32[3,2]{0,1:T(2,128)} %param.23) | copy-start | bytes 76
  0.7 0.7 %copy-start.1 = (f32[3,2]{0,1:T(2,128)S(1)}, f32[3,2]{0,1:T(2,128)}, u32[]{:S(2)}) copy-start(f32[3,2]{0,1:T(2,128)} %param.24) | copy-start | bytes 76

commit v2 on v1

--- a/solution.py
+++ b/solution.py
@@ -188,8 +188,11 @@
     query_s,
     mixed_s,
     mixed_rows_s,
-    resid_s,
     term_s,
+    block_sem,
+    i_send,
+    i_recv,
+    answer_s,
 ):
     me, mt = lax.axis_index("ep"), lax.axis_index("tp")
     total = ep * tp
@@ -201,6 +204,8 @@
     cache = key_w.shape[1]
     kv_local = key_w.shape[2] // head_size
     per_group = heads // kv_local
+    slots = f_send.shape[1]
+    key_tiles = i_send.shape[1] // LANES
     out_cols = out_ref.shape[1]
     f32, bf16 = jnp.float32, jnp.bfloat16
 
@@ -220,11 +225,10 @@
         loads[-1].start()
 
     barrier = pltpu.get_barrier_semaphore()
-    for step in range(1, total):
-        other = lax.rem(flat + step, total)
-        pl.semaphore_signal(
-            barrier, inc=1, device_id=(other // tp, lax.rem(other, tp)), device_id_type=MESH
-        )
+    greeted = [(lax.rem(me + step, ep), mt) for step in range(1, ep)]
+    greeted += [(me, lax.rem(mt + step, tp)) for step in range(1, tp)]
+    for device in greeted:
+        pl.semaphore_signal(barrier, inc=1, device_id=device, device_id_type=MESH)
 
     def send(phase, source, target, device):
         pltpu.make_async_remote_copy(
@@ -246,10 +250,27 @@
         a_send[e, 0] = normed[:, e * cols : (e + 1) * cols].astype(bf16)
         a_send[e, 1] = tokens_ref[:, e * cols : (e + 1) * cols]
     query_s[...] = jnp.zeros_like(query_s)
-    pl.semaphore_wait(barrier, total - 1)
+    keys_own = []
+    for row in range(batch):
+        for k in range(TOP):
+            slot = jnp.int32(0)
+            for past in range(row):
+                for other in range(TOP):
+                    slot += jnp.where(ids_ref[other, past] == ids_ref[k, row], 1, 0)
+            keys_own.append(ids_ref[k, row] * slots + slot)
+    lane = lax.broadcasted_iota(jnp.int32, (1, LANES * key_tiles), 1)
+    for k in range(TOP):
+        placed = jnp.zeros(lane.shape, jnp.int32)
+        for row in range(batch):
+            placed = jnp.where(lane == me * batch + row, keys_own[row * TOP + k], placed)
+        i_send[k : k + 1, :] = placed
+    pl.semaphore_wait(barrier, len(greeted))
     for peer in ep_peers():
         send(0, a_send.at[peer], a_recv.at[me], (peer, mt))
     a_recv[me] = a_send[me]
+    for peer in ep_peers():
+        send(6, i_send, i_recv.at[me], (peer, mt))
+    i_recv[me] = i_send[...]
 
     earlier = lax.broadcasted_iota(jnp.int32, (LANES, 2 * LANES), 0)
     later = lax.broadcasted_iota(jnp.int32, (LANES, 2 * LANES), 1)
@@ -263,16 +284,16 @@
         token_s[batch * e : batch * (e + 1), :] = a_recv[e, 1].astype(f32)
     part_s[...] = jnp.dot(rows_s[...].astype(bf16), query_w[...], preferred_element_type=f32)
     for e in range(ep):
-        b_send[e] = part_s[batch * e : batch * (e + 1), :]
+        b_send[e] = part_s[batch * e : batch * (e + 1), :].astype(bf16)
     for peer in ep_peers():
         send(1, b_send.at[peer], b_recv.at[me], (peer, mt))
     b_recv[me] = b_send[me]
     loads[1].wait()
     loads[2].wait()
     wait_bytes(b_recv, ep - 1, recv_sem.at[1])
-    query = b_recv[0]
+    query = b_recv[0].astype(f32)
     for e in range(1, ep):
-        query = query + b_recv[e]
+        query = query + b_recv[e].astype(f32)
     query = query.astype(bf16).astype(f32)
 
     groups = [(row, kv) for row in range(batch) for kv in range(kv_local)]
@@ -347,59 +368,102 @@
         resid = resid + d_recv[t].astype(f32)
     e_send[...] = resid.astype(bf16)
 
-    for peer in ep_peers():
-        send(4, e_send, e_recv.at[me], (peer, mt))
+    for step in range(1, ep):
+        pltpu.make_async_remote_copy(
+            src_ref=e_send,
+            dst_ref=e_recv.at[me],
+            send_sem=send_sem.at[4],
+            recv_sem=block_sem.at[me],
+            device_id=(lax.rem(me + step, ep), mt),
+            device_id_type=MESH,
+        ).start()
     e_recv[me] = e_send[...]
-    numbers = ids_ref[...]
-    routes = route_ref[...]
-    shares = [
-        jnp.sum(jnp.where(numbers == e, routes, 0.0), axis=1, keepdims=True) for e in range(ep)
-    ]
+
+    wait_bytes(i_recv, ep - 1, recv_sem.at[6])
+    keys_all = i_recv[0]
+    for e in range(1, ep):
+        keys_all = keys_all + i_recv[e]
+    rows = ep * batch
+    pack_rows = lax.broadcasted_iota(jnp.int32, (ep * slots, rows), 0)
+    pack_cols = lax.broadcasted_iota(jnp.int32, (ep * slots, rows), 1)
+    row_owner = jnp.zeros_like(pack_rows)
+    col_owner = jnp.zeros_like(pack_cols)
+    for e in range(1, ep):
+        row_owner = row_owner + jnp.where(pack_rows >= e * slots, 1, 0)
+        col_owner = col_owner + jnp.where(pack_cols >= e * batch, 1, 0)
+    wanted = pack_rows - row_owner * slots + me * slots
+    named = wanted == keys_all[0:1, :rows]
+    for k in range(1, TOP):
+        named = named | (wanted == keys_all[k : k + 1, :rows])
+    pack = jnp.where(named & (row_owner == col_owner), 1.0, 0.0).astype(bf16)
+    pick_rows = lax.broadcasted_iota(jnp.int32, (batch, ep * slots), 0)
+    pick_cols = lax.broadcasted_iota(jnp.int32, (batch, ep * slots), 1)
+    line = lax.broadcasted_iota(jnp.int32, (batch, 1), 0)
+    picks, routes = [], []
+    for k in range(TOP):
+        chosen = jnp.zeros_like(pick_rows)
+        route = jnp.zeros((batch, 1), f32)
+        for row in range(batch):
+            chosen = jnp.where(pick_rows == row, keys_own[row * TOP + k], chosen)
+            route = jnp.where(line == row, route_ref[k, row], route)
+        picks.append(jnp.where(pick_cols == chosen, 1.0, 0.0).astype(bf16))
+        routes.append(route)
+    row_at = lax.broadcasted_iota(jnp.int32, (batch, rows), 0) + me * batch
+    column_at = lax.broadcasted_iota(jnp.int32, (batch, rows), 1)
+    own_rows = (row_at == column_at).astype(f32).astype(bf16)
+
     loads[4].wait()
     loads[5].wait()
     loads[6].wait()
-    wait_bytes(e_recv, ep - 1, recv_sem.at[4])
-    square = None
-    for e in range(ep):
-        block = e_recv[e].astype(f32)
-        resid_s[e] = block
-        square = block * block if square is None else square + block * block
-    scale = lax.rsqrt(jnp.sum(square, axis=-1, keepdims=True) / width + 1e-06)
-    normed2 = jnp.concatenate(
-        [
-            (resid_s[e] * scale * expert_gain_ref[:, e * cols : (e + 1) * cols]).astype(bf16)
-            for e in range(ep)
-        ],
-        axis=1,
-    )
-    gate = jnp.dot(normed2, gate_w[0], preferred_element_type=f32)
-    upward = jnp.dot(normed2, up_w[0], preferred_element_type=f32)
+    order = [0]
+    for step in range(1, ep // 2 + 1):
+        order += [step, ep - step]
+    square = gate = upward = None
+    for step in list(dict.fromkeys(order))[:ep]:
+        source = lax.rem(me + step, ep)
+        if step:
+            pltpu.make_async_copy(e_send, e_recv.at[source], block_sem.at[source]).wait()
+        first = pl.multiple_of(source * cols, cols)
+        block = e_recv[source].astype(f32)
+        scaled = (block * expert_gain_ref[:, pl.ds(first, cols)]).astype(bf16)
+        terms = (
+            jnp.sum(block * block, axis=-1, keepdims=True),
+            jnp.dot(scaled, gate_w[0, pl.ds(first, cols), :], preferred_element_type=f32),
+            jnp.dot(scaled, up_w[0, pl.ds(first, cols), :], preferred_element_type=f32),
+        )
+        if square is None:
+            square, gate, upward = terms
+        else:
+            square, gate, upward = square + terms[0], gate + terms[1], upward + terms[2]
+    scale = lax.rsqrt(square / width + 1e-06)
+    gate, upward = gate * scale, upward * scale
     hidden = (gate / (1.0 + jnp.exp(-gate)) * upward).astype(bf16)
-    term_s[...] = jnp.dot(hidden, down_w[0], preferred_element_type=f32)
+    packed = jnp.dot(pack, hidden, preferred_element_type=f32).astype(bf16)
+    term_s[...] = jnp.dot(packed, down_w[0], preferred_element_type=f32)
     for e in range(ep):
         for t in range(tp):
             f_send[e * tp + t] = term_s[
-                batch * e : batch * (e + 1), t * out_cols : (t + 1) * out_cols
+                slots * e : slots * (e + 1), t * out_cols : (t + 1) * out_cols
             ].astype(bf16)
     for step in range(1, total):
         other = lax.rem(flat + step, total)
         send(5, f_send.at[other], f_recv.at[flat], (other // tp, lax.rem(other, tp)))
     f_recv[flat] = f_send[flat]
     own_blocks = out_cols // cols
-    row_at = lax.broadcasted_iota(jnp.int32, (batch, ep * batch), 0) + me * batch
-    column_at = lax.broadcasted_iota(jnp.int32, (batch, ep * batch), 1)
-    own_rows = (row_at == column_at).astype(f32).astype(bf16)
     own_resid = jnp.concatenate(
         [e_recv[mt * own_blocks + j] for j in range(own_blocks)], axis=1
     )
     result = jnp.dot(own_rows, own_resid, preferred_element_type=f32)
     wait_bytes(f_recv, total - 1, recv_sem.at[5])
-    mixture = jnp.zeros_like(result)
     for e in range(ep):
         summed = f_recv[e * tp].astype(f32)
         for t in range(1, tp):
             summed = summed + f_recv[e * tp + t].astype(f32)
-        mixture = mixture + summed.astype(bf16).astype(f32) * shares[e]
+        answer_s[slots * e : slots * (e + 1), :] = summed
+    answers = answer_s[...].astype(bf16)
+    mixture = jnp.zeros_like(result)
+    for pick, route in zip(picks, routes):
+        mixture = mixture + route * jnp.dot(pick, answers, preferred_element_type=f32)
     out_ref[...] = (result + mixture).astype(bf16)
 
     wait_bytes(a_recv, ep - 1, send_sem.at[0])
@@ -407,6 +471,7 @@
     wait_bytes(c_recv, ep - 1, send_sem.at[2])
     wait_bytes(d_recv, tp - 1, send_sem.at[3])
     wait_bytes(e_recv, ep - 1, send_sem.at[4])
+    wait_bytes(i_recv, ep - 1, send_sem.at[6])
     wait_bytes(f_recv, total - 1, send_sem.at[5])
 
 
@@ -431,6 +496,9 @@
     cols, heads_width = query_weight.shape
     out_cols = width // tp
     rows = ep * batch
+    groups = ep // EPG
+    slots = max(2, (batch + groups - 1) // groups)
+    key_lanes = (rows + LANES - 1) // LANES * LANES
     heads = head_offset.shape[0]
     cache, kv_local, head_size = key_cache.shape[1:]
     keys = key_cache.reshape(batch, cache, kv_local * head_size)
@@ -446,34 +514,37 @@
 
     return pl.pallas_call(
         body,
-        out_shape=jax.ShapeDtypeStruct((batch, out_cols), bf16),
-        in_specs=[vmem, vmem, vmem, smem, smem, vmem, vmem] + [hbm] * len(big),
+        out_shape=pltpu.VMEM((batch, out_cols), bf16),
+        in_specs=[vmem, vmem, vmem, smem, smem, smem, smem] + [hbm] * len(big),
         out_specs=vmem,
         scratch_shapes=[pltpu.VMEM(array.shape, array.dtype) for array in big]
         + [
             pltpu.SemaphoreType.DMA((len(big),)),
-            pltpu.SemaphoreType.DMA((6,)),
-            pltpu.SemaphoreType.DMA((6,)),
+            pltpu.SemaphoreType.DMA((7,)),
+            pltpu.SemaphoreType.DMA((7,)),
             pltpu.VMEM((ep, 2, batch, cols), bf16),
             pltpu.VMEM((ep, 2, batch, cols), bf16),
-            pltpu.VMEM((ep, batch, heads_width), f32),
-            pltpu.VMEM((ep, batch, heads_width), f32),
+            pltpu.VMEM((ep, batch, heads_width), bf16),
+            pltpu.VMEM((ep, batch, heads_width), bf16),
             pltpu.VMEM((batch, heads_width), bf16),
             pltpu.VMEM((ep, batch, heads_width), bf16),
             pltpu.VMEM((rows, cols), bf16),
             pltpu.VMEM((tp, rows, cols), bf16),
             pltpu.VMEM((rows, cols), bf16),
             pltpu.VMEM((ep, rows, cols), bf16),
-            pltpu.VMEM((ep * tp, batch, out_cols), bf16),
-            pltpu.VMEM((ep * tp, batch, out_cols), bf16),
+            pltpu.VMEM((ep * tp, slots, out_cols), bf16),
+            pltpu.VMEM((ep * tp, slots, out_cols), bf16),
             pltpu.VMEM((rows, cols), f32),
             pltpu.VMEM((rows, cols), f32),
             pltpu.VMEM((rows, heads_width), f32),
             pltpu.VMEM((batch, kv_local, SUBLANES, head_size), f32),
             pltpu.VMEM((batch, heads_width), f32),
             pltpu.VMEM((rows, heads_width), f32),
-            pltpu.VMEM((ep, rows, cols), f32),
-            pltpu.VMEM((rows, width), f32),
+            pltpu.VMEM((ep * slots, width), f32),
+            pltpu.SemaphoreType.DMA((ep,)),
+            pltpu.VMEM((TOP, key_lanes), jnp.int32),
+            pltpu.VMEM((ep, TOP, key_lanes), jnp.int32),
+            pltpu.VMEM((ep * slots, out_cols), f32),
         ],
         compiler_params=pltpu.CompilerParams(
             collective_id=0, has_side_effects=True, vmem_limit_bytes=60 * 1024 * 1024
@@ -484,8 +555,8 @@
         expert_gain.reshape(1, width),
         seq_lengths,
         head_offset,
-        expert_ids,
-        route_weight,
+        expert_ids.T,
+        route_weight.T,
         *big,
     )
 

time: 37.3 us -> 33.6 us (0.901)
  local copies, waits for them, and re-layouts: 3.28 us -> 0.6 us
  Pallas kernels: 33.7 us -> 32.8 us
    unnamed x7 -> x1, local copies, waits for them, and re-layouts: 3.28 us -> 0.6 us
    pallas_call x1, Pallas kernels: 33.7 us -> 32.8 us  [local_kernel(): pl.pallas_call(body, out_shape=pltpu.VMEM((batch, out_cols), bf16), in_sp...]
where the time goes in v2:
time: 33.6 us; the launch traced here: 33.4 us
  Pallas kernels  32.8 us (98%)
  local copies, waits for them, and re-layouts  0.6 us (2%)
    pallas_call x1, Pallas kernels, local_kernel(): pl.pallas_call(body, out_shape=pltpu.VMEM((batch, out_cols), bf16), in_sp...  32.8 us

profile of v2, /device:TPU:0, one launch (start us, length us, event | category | flops | bytes accessed | tf_op | source)
XLA Modules:
  0.0 33.4 jit_solution(12184051814673543275)
XLA Ops:
  0.0 32.8 %shard_map.136 = bf16[3,512]{1,0:T(4,128)(2,1)S(1)} custom-call(bf16[3,2048]{1,0:T(4,128)(2,1)} %refs_0_.1, f32[1,2048]{1,0:T(1,128)} %bitcast.8, f32[1,2048]{1,0:T(1,128)} %bitcast.9, s32[3]{0:T(128)} %refs_3_.1, f32[4]{0:T(128)} %refs_4_.1, s32[2,3]{1,0:T(2,128)} %bitcast.10, f32[2,3]{1,0:T(2,128)} %bitcast.11, bf16[256,512]{1,0:T(8,128)(2,1)} %refs_7_.1, ...), custom_call_target="tpu_custom_call" | custom-call | tf_op jit(solution)/shard_map/pallas_call | solution.py:515
  32.8 0.6 %copy.16 = bf16[3,512]{1,0:T(4,128)(2,1)} copy(bf16[3,512]{1,0:T(4,128)(2,1)S(1)} %shard_map.136) | data formatting | bytes 6144
